TPU v7x, 32 devices: a whole 2x2x4 slice. The times are simulated.
32 devices in a mesh: sp: 8 (over z, x), tp: 4 (over y, core).
Axes of the slice: x: 2, y: 2, z: 4, core: 2. Of those that a mesh axis runs over, the one named last changes fastest.
Arguments:
- tokens: bfloat16 [8192, 4096], P(('sp', 'tp')), may hold values from -6 to 6
- norm_gain: float32 [4096], replicated, may hold values from 0.1 to 1.9
- q_down: bfloat16 [4096, 768], replicated, may hold values from -0.09375 to 0.09375
- kv_down: bfloat16 [4096, 512], replicated, may hold values from -0.09375 to 0.09375
- rope_down: bfloat16 [4096, 32], replicated, may hold values from -8 to 8
- q_gain: float32 [768], replicated, may hold values from 0.1 to 1.9
- kv_gain: float32 [512], replicated, may hold values from 0.1 to 1.9
- q_up: bfloat16 [768, 1536], P(None, 'tp'), may hold values from -0.21875 to 0.21875
- kv_up: bfloat16 [512, 2048], P(None, 'tp'), may hold values from -0.25 to 0.25
- out_weight: bfloat16 [1024, 4096], replicated, may hold values from -0.1875 to 0.1875
- out_gain: float32 [4096], replicated, may hold values from 0.1 to 1.9
Outputs:
- mixed: bfloat16 [8192, 4096], P(('sp', 'tp'))
All inputs are finite; a program needn't handle non-finite values.
Results may differ from a plain program's by a relative error of at most 0.02.
The roundings to bfloat16 on the way count: a program that leaves them out, or rounds other values in their place, can miss the bound.
Values may be sent and summed in bfloat16 or wider, within the bound.
A program may use at most 128 MiB of HBM per device.

v0:
```python
import jax
import jax.numpy as jnp
from jax import lax
from jax.sharding import PartitionSpec as P

NOPE = 64
ROPE = 32
VDIM = 64
EPS = 1e-06
THETA = 500000.0


def scaled_norm(values_in, gain):
    values_in = values_in.astype(jnp.float32)
    return (
        values_in * lax.rsqrt(jnp.mean(values_in * values_in, axis=-1, keepdims=True) + EPS) * gain
    )


def rotate(values_in, position):
    width = values_in.shape[-1]
    half_dim = width // 2
    inverse = 1.0 / THETA ** (jnp.arange(0, width, 2, dtype=jnp.float32) / width)
    angles = position[:, None] * inverse[None, :]
    angles = angles.reshape((angles.shape[0],) + (1,) * (values_in.ndim - 2) + (half_dim,))
    cosine = jnp.cos(angles)
    sine = jnp.sin(angles)
    left = values_in[..., :half_dim]
    right = values_in[..., half_dim:]
    return jnp.concatenate([left * cosine - right * sine, right * cosine + left * sine], axis=-1)


def local(
    tokens,
    norm_gain,
    q_down,
    kv_down,
    rope_down,
    q_gain,
    kv_gain,
    q_up,
    kv_up,
    out_weight,
    out_gain,
):
    row_count = tokens.shape[0]
    tp_count = lax.axis_size("tp")
    tp_place = lax.axis_index("tp")
    sp_place = lax.axis_index("sp")
    group_rows = row_count * tp_count
    row_first = (sp_place * tp_count + tp_place) * row_count
    own_position = (row_first + jnp.arange(row_count)).astype(jnp.float32)
    normed = scaled_norm(tokens, norm_gain).astype(jnp.bfloat16)
    q_lat = scaled_norm(jnp.dot(normed, q_down, preferred_element_type=jnp.float32), q_gain).astype(
        jnp.bfloat16
    )
    kv_lat = scaled_norm(
        jnp.dot(normed, kv_down, preferred_element_type=jnp.float32), kv_gain
    ).astype(jnp.bfloat16)
    key_rot = rotate(
        jnp.dot(normed, rope_down, preferred_element_type=jnp.float32), own_position
    ).astype(jnp.bfloat16)
    q_group, kv_group, rot_group = (
        lax.all_gather(q_lat, "tp", axis=0, tiled=True),
        lax.all_gather(kv_lat, "tp", axis=0, tiled=True),
        lax.all_gather(key_rot, "tp", axis=0, tiled=True),
    )
    query_first = sp_place * group_rows
    query_index = query_first + jnp.arange(group_rows)
    head_count = q_up.shape[1] // (NOPE + ROPE)
    query = jnp.dot(q_group, q_up, preferred_element_type=jnp.float32).reshape(
        group_rows, head_count, NOPE + ROPE
    )
    query = jnp.concatenate(
        [query[..., :NOPE], rotate(query[..., NOPE:], query_index.astype(jnp.float32))], axis=-1
    )
    query = query.astype(jnp.bfloat16)
    query_nope = query[..., :NOPE]
    query_rot = query[..., NOPE:]
    factor = (NOPE + ROPE) ** (-0.5)

    def attend_block(state, key_rows, rot_rows, block_first):

        def compute(state_in):
            top_score, total, summed = state_in
            keys_values = jnp.dot(key_rows, kv_up, preferred_element_type=jnp.float32).astype(
                jnp.bfloat16
            )
            keys_values = keys_values.reshape(key_rows.shape[0], head_count, NOPE + VDIM)
            scores = jnp.einsum(
                "qhd,khd->hqk",
                query_nope,
                keys_values[..., :NOPE],
                preferred_element_type=jnp.float32,
            )
            scores = scores + jnp.einsum(
                "qhd,kd->hqk", query_rot, rot_rows, preferred_element_type=jnp.float32
            )
            scores = scores * factor
            key_index = block_first + jnp.arange(key_rows.shape[0])
            visible = (key_index[None, :] <= query_index[:, None])[None]
            scores = jnp.where(visible, scores, -1e30)
            new_top = jnp.maximum(top_score, jnp.max(scores, axis=-1))
            correction = jnp.exp(top_score - new_top)
            weights = jnp.where(visible, jnp.exp(scores - new_top[..., None]), 0.0)
            total_new = total * correction + jnp.sum(weights, axis=-1)
            product = jnp.einsum(
                "hqk,khd->hqd",
                weights.astype(jnp.bfloat16),
                keys_values[..., NOPE:],
                preferred_element_type=jnp.float32,
            )
            return (new_top, total_new, summed * correction[..., None] + product)

        return lax.cond(
            block_first <= query_first + group_rows - 1, compute, lambda state_in: state_in, state
        )

    start_state = (
        jnp.full((head_count, group_rows), -1e30, jnp.float32),
        jnp.zeros((head_count, group_rows), jnp.float32),
        jnp.zeros((head_count, group_rows, VDIM), jnp.float32),
    )
    key_piece = lax.all_gather(kv_group, "sp", axis=0, tiled=True)
    rot_piece = lax.all_gather(rot_group, "sp", axis=0, tiled=True)
    piece_rows = rot_piece.shape[0]
    block_count = piece_rows // group_rows
    key_blocks = key_piece.reshape((block_count, group_rows) + key_piece.shape[1:])
    rot_blocks = rot_piece.reshape(block_count, group_rows, rot_piece.shape[1])

    def step(state_in, index):
        block_first = index * group_rows
        return (attend_block(state_in, key_blocks[index], rot_blocks[index], block_first), None)

    state_out, unused = lax.scan(step, start_state, jnp.arange(block_count))
    top_score, total, summed = state_out
    attended = (summed / total[..., None]).transpose(1, 0, 2).reshape(group_rows, head_count * VDIM)
    attended = attended.astype(jnp.bfloat16)
    own_heads = lax.all_to_all(attended, "tp", split_axis=0, concat_axis=1, tiled=True)
    projected = jnp.dot(own_heads, out_weight, preferred_element_type=jnp.float32)
    return scaled_norm(projected, out_gain).astype(jnp.bfloat16)


def solution(mesh):
    return jax.shard_map(
        local,
        mesh=mesh,
        in_specs=(
            P(("sp", "tp"), None),
            P(),
            P(),
            P(),
            P(),
            P(),
            P(),
            P(None, "tp"),
            P(None, "tp"),
            P(),
            P(),
        ),
        out_specs=P(("sp", "tp"), None),
        check_vma=False,
    )
```

profile of v0, /device:TPU:26, one launch (start us, length us, event | category | flops | bytes accessed | tf_op | source)
XLA Modules:
  0.0 503.1 jit_solution(1699244683318475322)
XLA Ops:
  19.8 12.0 %all-gather.4.cloned.1.call-done = bf16[1024,512]{1,0:T(8,128)(2,1)} async-done(((bf16[256,512]{1,0:T(8,128)(2,1)}), bf16[1024,512]{1,0:T(8,128)(2,1)}) %all-gather.4.cloned.1.call-update) | async-done | bytes 1048592 | tf_op jit(solution)/shard_map/all_gather | solution.py:65
  38.0 32.3 %all_gather.19 = bf16[8192,32]{0,1:T(8,128)(2,1)S(1)} all-gather(bf16[1024,32]{0,1:T(8,128)(2,1)S(1)} %all_gather.18), channel_id=1, replica_groups=mesh['sp'=8,'tp'=4] {'sp'}, dimensions={0}, use_global_device_ids=true | all-gather | bytes 589824 | tf_op jit(solution)/shard_map/all_gather | solution.py:125
  73.9 102.8 %all-gather.6.cloned.1.call-done = bf16[8192,512]{1,0:T(8,128)(2,1)} async-done(((bf16[1024,512]{1,0:T(8,128)(2,1)}), bf16[8192,512]{1,0:T(8,128)(2,1)}) %all-gather.6.cloned.1.call-update) | async-done | bytes 8388624 | tf_op jit(solution)/shard_map/all_gather | solution.py:124
  177.9 297.7 %while.17 = (s32[]{:T(128)}, f32[4,1024]{1,0:T(4,128)S(1)}, f32[4,1024]{1,0:T(4,128)S(1)}, f32[4,1024,64]{1,2,0:T(8,128)}, s32[8]{0:T(128)S(1)}, /*index=5*/s32[...) while((s32[]{:T(128)}, f32[4,1024]{1,0:T(4,128)S(1)}, ...), condition=%wide.region_8.9_spmd.clone, body=%wide.region_3.8_spmd.clone.sunk | while | flops 1923098624 | bytes 107569616 | solution.py:135
  179.0 36.1 %conditional.3 = ((f32[4,1024]{1,0:T(4,128)S(1)}, f32[4,1024]{1,0:T(4,128)S(1)}, f32[4,1024,64]{1,2,0:T(8,128)})) conditional(s32[]{:T(128)} %convert_element_type.106, (f32[4,1024]{1,0:T(4,128)S(1)}, f32[4,1024]{1,0:T(4,128)S(1)}, f32[4,1024,64]{1,2,0:T(8,128)}) %tuple.62, (s32[]{:T(128)}, s32[]{:T(128)}, s32[]{:T(128)}, ...), branch_computations={%region_4.4_spmd, %region_5.7_spmd} | conditional | flops 1923098624 | bytes 107565224 | solution.py:115
  187.9 9.2 %fusion.40 = (f32[4,1024]{1,0:T(4,128)S(1)}, f32[4,1024,1024]{1,2,0:T(8,128)}) fusion(bf16[1024,4,32]{0,2,1:T(8,128)(2,1)S(1)} %get-tuple-element.258, bf16[8,1024,32]{1,2,0:T(8,128)(2,1)} %get-tuple-element.257, s32[]{:T(128)S(6)} %select_n.18, f32[4,1024,1024]{2,1,0:T(8,128)S(1)} %fusion.15, pred[1024,1024]{0,1:T(8,128)(4,1)} %broadcast_compare_fusion), kind=kOutput, calls=%fused_computation.67 | convolution fusion | flops 285208576 | bytes 34947076 | tf_op jit(solution)/shard_map/while/body/eval_jaxpr/cond/branch_1_fun/qhd,kd->hqk/dot_general | solution.py:96
  197.1 9.2 %fusion.5 = f32[4,1024]{1,0:T(4,128)S(1)} fusion(f32[4,1024,1024]{1,2,0:T(8,128)} %get-tuple-element.389, f32[4,1024]{1,0:T(4,128)S(1)} %max.5, pred[1024,1024]{0,1:T(8,128)(4,1)} %broadcast_compare_fusion), kind=kLoop, calls=%fused_computation.6 | loop fusion | flops 12578816 | bytes 17858560 | tf_op jit(solution)/shard_map/while/body/eval_jaxpr/cond/branch_1_fun/reduce_sum | solution.py:106
  206.3 8.8 %fusion.9 = f32[4,1024,64]{1,2,0:T(8,128)} fusion(f32[4,1024,1024]{1,2,0:T(8,128)} %get-tuple-element.389, f32[4,1024]{1,0:T(4,128)S(1)} %max.5, pred[1024,1024]{0,1:T(8,128)(4,1)S(1)} %copy-done.2, f32[4,1024,64]{1,2,0:T(8,128)} %get-tuple-element.260, bf16[1024,4,128]{0,2,1:T(8,128)(2,1)S(1)} %bitcast.45, f32[4,1024]{1,0:T(4,128)S(1)} %get-tuple-element.387), kind=kOutput, calls=%fused_computation.11 | convolution fusion | flops 549978112 | bytes 20480000 | tf_op jit(solution)/shard_map/while/body/eval_jaxpr/cond/branch_1_fun/hqk,khd->hqd/dot_general | solution.py:107
  216.2 36.1 %conditional.3 = ((f32[4,1024]{1,0:T(4,128)S(1)}, f32[4,1024]{1,0:T(4,128)S(1)}, f32[4,1024,64]{1,2,0:T(8,128)})) conditional(s32[]{:T(128)} %convert_element_type.106, (f32[4,1024]{1,0:T(4,128)S(1)}, f32[4,1024]{1,0:T(4,128)S(1)}, f32[4,1024,64]{1,2,0:T(8,128)}) %tuple.62, (s32[]{:T(128)}, s32[]{:T(128)}, s32[]{:T(128)}, ...), branch_computations={%region_4.4_spmd, %region_5.7_spmd} | conditional | flops 1923098624 | bytes 107565224 | solution.py:115
  225.2 9.2 %fusion.40 = (f32[4,1024]{1,0:T(4,128)S(1)}, f32[4,1024,1024]{1,2,0:T(8,128)}) fusion(bf16[1024,4,32]{0,2,1:T(8,128)(2,1)S(1)} %get-tuple-element.258, bf16[8,1024,32]{1,2,0:T(8,128)(2,1)} %get-tuple-element.257, s32[]{:T(128)S(6)} %select_n.18, f32[4,1024,1024]{2,1,0:T(8,128)S(1)} %fusion.15, pred[1024,1024]{0,1:T(8,128)(4,1)} %broadcast_compare_fusion), kind=kOutput, calls=%fused_computation.67 | convolution fusion | flops 285208576 | bytes 34947076 | tf_op jit(solution)/shard_map/while/body/eval_jaxpr/cond/branch_1_fun/qhd,kd->hqk/dot_general | solution.py:96
  234.3 9.2 %fusion.5 = f32[4,1024]{1,0:T(4,128)S(1)} fusion(f32[4,1024,1024]{1,2,0:T(8,128)} %get-tuple-element.389, f32[4,1024]{1,0:T(4,128)S(1)} %max.5, pred[1024,1024]{0,1:T(8,128)(4,1)} %broadcast_compare_fusion), kind=kLoop, calls=%fused_computation.6 | loop fusion | flops 12578816 | bytes 17858560 | tf_op jit(solution)/shard_map/while/body/eval_jaxpr/cond/branch_1_fun/reduce_sum | solution.py:106
  253.5 36.1 %conditional.3 = ((f32[4,1024]{1,0:T(4,128)S(1)}, f32[4,1024]{1,0:T(4,128)S(1)}, f32[4,1024,64]{1,2,0:T(8,128)})) conditional(s32[]{:T(128)} %convert_element_type.106, (f32[4,1024]{1,0:T(4,128)S(1)}, f32[4,1024]{1,0:T(4,128)S(1)}, f32[4,1024,64]{1,2,0:T(8,128)}) %tuple.62, (s32[]{:T(128)}, s32[]{:T(128)}, s32[]{:T(128)}, ...), branch_computations={%region_4.4_spmd, %region_5.7_spmd} | conditional | flops 1923098624 | bytes 107565224 | solution.py:115
  262.4 9.2 %fusion.40 = (f32[4,1024]{1,0:T(4,128)S(1)}, f32[4,1024,1024]{1,2,0:T(8,128)}) fusion(bf16[1024,4,32]{0,2,1:T(8,128)(2,1)S(1)} %get-tuple-element.258, bf16[8,1024,32]{1,2,0:T(8,128)(2,1)} %get-tuple-element.257, s32[]{:T(128)S(6)} %select_n.18, f32[4,1024,1024]{2,1,0:T(8,128)S(1)} %fusion.15, pred[1024,1024]{0,1:T(8,128)(4,1)} %broadcast_compare_fusion), kind=kOutput, calls=%fused_computation.67 | convolution fusion | flops 285208576 | bytes 34947076 | tf_op jit(solution)/shard_map/while/body/eval_jaxpr/cond/branch_1_fun/qhd,kd->hqk/dot_general | solution.py:96
  271.6 9.2 %fusion.5 = f32[4,1024]{1,0:T(4,128)S(1)} fusion(f32[4,1024,1024]{1,2,0:T(8,128)} %get-tuple-element.389, f32[4,1024]{1,0:T(4,128)S(1)} %max.5, pred[1024,1024]{0,1:T(8,128)(4,1)} %broadcast_compare_fusion), kind=kLoop, calls=%fused_computation.6 | loop fusion | flops 12578816 | bytes 17858560 | tf_op jit(solution)/shard_map/while/body/eval_jaxpr/cond/branch_1_fun/reduce_sum | solution.py:106
  290.7 36.1 %conditional.3 = ((f32[4,1024]{1,0:T(4,128)S(1)}, f32[4,1024]{1,0:T(4,128)S(1)}, f32[4,1024,64]{1,2,0:T(8,128)})) conditional(s32[]{:T(128)} %convert_element_type.106, (f32[4,1024]{1,0:T(4,128)S(1)}, f32[4,1024]{1,0:T(4,128)S(1)}, f32[4,1024,64]{1,2,0:T(8,128)}) %tuple.62, (s32[]{:T(128)}, s32[]{:T(128)}, s32[]{:T(128)}, ...), branch_computations={%region_4.4_spmd, %region_5.7_spmd} | conditional | flops 1923098624 | bytes 107565224 | solution.py:115
  299.6 9.2 %fusion.40 = (f32[4,1024]{1,0:T(4,128)S(1)}, f32[4,1024,1024]{1,2,0:T(8,128)}) fusion(bf16[1024,4,32]{0,2,1:T(8,128)(2,1)S(1)} %get-tuple-element.258, bf16[8,1024,32]{1,2,0:T(8,128)(2,1)} %get-tuple-element.257, s32[]{:T(128)S(6)} %select_n.18, f32[4,1024,1024]{2,1,0:T(8,128)S(1)} %fusion.15, pred[1024,1024]{0,1:T(8,128)(4,1)} %broadcast_compare_fusion), kind=kOutput, calls=%fused_computation.67 | convolution fusion | flops 285208576 | bytes 34947076 | tf_op jit(solution)/shard_map/while/body/eval_jaxpr/cond/branch_1_fun/qhd,kd->hqk/dot_general | solution.py:96
  308.8 9.2 %fusion.5 = f32[4,1024]{1,0:T(4,128)S(1)} fusion(f32[4,1024,1024]{1,2,0:T(8,128)} %get-tuple-element.389, f32[4,1024]{1,0:T(4,128)S(1)} %max.5, pred[1024,1024]{0,1:T(8,128)(4,1)} %broadcast_compare_fusion), kind=kLoop, calls=%fused_computation.6 | loop fusion | flops 12578816 | bytes 17858560 | tf_op jit(solution)/shard_map/while/body/eval_jaxpr/cond/branch_1_fun/reduce_sum | solution.py:106
  318.0 8.8 %fusion.9 = f32[4,1024,64]{1,2,0:T(8,128)} fusion(f32[4,1024,1024]{1,2,0:T(8,128)} %get-tuple-element.389, f32[4,1024]{1,0:T(4,128)S(1)} %max.5, pred[1024,1024]{0,1:T(8,128)(4,1)S(1)} %copy-done.2, f32[4,1024,64]{1,2,0:T(8,128)} %get-tuple-element.260, bf16[1024,4,128]{0,2,1:T(8,128)(2,1)S(1)} %bitcast.45, f32[4,1024]{1,0:T(4,128)S(1)} %get-tuple-element.387), kind=kOutput, calls=%fused_computation.11 | convolution fusion | flops 549978112 | bytes 20480000 | tf_op jit(solution)/shard_map/while/body/eval_jaxpr/cond/branch_1_fun/hqk,khd->hqd/dot_general | solution.py:107
  327.9 36.1 %conditional.3 = ((f32[4,1024]{1,0:T(4,128)S(1)}, f32[4,1024]{1,0:T(4,128)S(1)}, f32[4,1024,64]{1,2,0:T(8,128)})) conditional(s32[]{:T(128)} %convert_element_type.106, (f32[4,1024]{1,0:T(4,128)S(1)}, f32[4,1024]{1,0:T(4,128)S(1)}, f32[4,1024,64]{1,2,0:T(8,128)}) %tuple.62, (s32[]{:T(128)}, s32[]{:T(128)}, s32[]{:T(128)}, ...), branch_computations={%region_4.4_spmd, %region_5.7_spmd} | conditional | flops 1923098624 | bytes 107565224 | solution.py:115
  336.8 9.2 %fusion.40 = (f32[4,1024]{1,0:T(4,128)S(1)}, f32[4,1024,1024]{1,2,0:T(8,128)}) fusion(bf16[1024,4,32]{0,2,1:T(8,128)(2,1)S(1)} %get-tuple-element.258, bf16[8,1024,32]{1,2,0:T(8,128)(2,1)} %get-tuple-element.257, s32[]{:T(128)S(6)} %select_n.18, f32[4,1024,1024]{2,1,0:T(8,128)S(1)} %fusion.15, pred[1024,1024]{0,1:T(8,128)(4,1)} %broadcast_compare_fusion), kind=kOutput, calls=%fused_computation.67 | convolution fusion | flops 285208576 | bytes 34947076 | tf_op jit(solution)/shard_map/while/body/eval_jaxpr/cond/branch_1_fun/qhd,kd->hqk/dot_general | solution.py:96
  346.0 9.2 %fusion.5 = f32[4,1024]{1,0:T(4,128)S(1)} fusion(f32[4,1024,1024]{1,2,0:T(8,128)} %get-tuple-element.389, f32[4,1024]{1,0:T(4,128)S(1)} %max.5, pred[1024,1024]{0,1:T(8,128)(4,1)} %broadcast_compare_fusion), kind=kLoop, calls=%fused_computation.6 | loop fusion | flops 12578816 | bytes 17858560 | tf_op jit(solution)/shard_map/while/body/eval_jaxpr/cond/branch_1_fun/reduce_sum | solution.py:106
  365.1 36.1 %conditional.3 = ((f32[4,1024]{1,0:T(4,128)S(1)}, f32[4,1024]{1,0:T(4,128)S(1)}, f32[4,1024,64]{1,2,0:T(8,128)})) conditional(s32[]{:T(128)} %convert_element_type.106, (f32[4,1024]{1,0:T(4,128)S(1)}, f32[4,1024]{1,0:T(4,128)S(1)}, f32[4,1024,64]{1,2,0:T(8,128)}) %tuple.62, (s32[]{:T(128)}, s32[]{:T(128)}, s32[]{:T(128)}, ...), branch_computations={%region_4.4_spmd, %region_5.7_spmd} | conditional | flops 1923098624 | bytes 107565224 | solution.py:115
  374.0 9.2 %fusion.40 = (f32[4,1024]{1,0:T(4,128)S(1)}, f32[4,1024,1024]{1,2,0:T(8,128)}) fusion(bf16[1024,4,32]{0,2,1:T(8,128)(2,1)S(1)} %get-tuple-element.258, bf16[8,1024,32]{1,2,0:T(8,128)(2,1)} %get-tuple-element.257, s32[]{:T(128)S(6)} %select_n.18, f32[4,1024,1024]{2,1,0:T(8,128)S(1)} %fusion.15, pred[1024,1024]{0,1:T(8,128)(4,1)} %broadcast_compare_fusion), kind=kOutput, calls=%fused_computation.67 | convolution fusion | flops 285208576 | bytes 34947076 | tf_op jit(solution)/shard_map/while/body/eval_jaxpr/cond/branch_1_fun/qhd,kd->hqk/dot_general | solution.py:96
  383.2 9.2 %fusion.5 = f32[4,1024]{1,0:T(4,128)S(1)} fusion(f32[4,1024,1024]{1,2,0:T(8,128)} %get-tuple-element.389, f32[4,1024]{1,0:T(4,128)S(1)} %max.5, pred[1024,1024]{0,1:T(8,128)(4,1)} %broadcast_compare_fusion), kind=kLoop, calls=%fused_computation.6 | loop fusion | flops 12578816 | bytes 17858560 | tf_op jit(solution)/shard_map/while/body/eval_jaxpr/cond/branch_1_fun/reduce_sum | solution.py:106
  392.4 8.8 %fusion.9 = f32[4,1024,64]{1,2,0:T(8,128)} fusion(f32[4,1024,1024]{1,2,0:T(8,128)} %get-tuple-element.389, f32[4,1024]{1,0:T(4,128)S(1)} %max.5, pred[1024,1024]{0,1:T(8,128)(4,1)S(1)} %copy-done.2, f32[4,1024,64]{1,2,0:T(8,128)} %get-tuple-element.260, bf16[1024,4,128]{0,2,1:T(8,128)(2,1)S(1)} %bitcast.45, f32[4,1024]{1,0:T(4,128)S(1)} %get-tuple-element.387), kind=kOutput, calls=%fused_computation.11 | convolution fusion | flops 549978112 | bytes 20480000 | tf_op jit(solution)/shard_map/while/body/eval_jaxpr/cond/branch_1_fun/hqk,khd->hqd/dot_general | solution.py:107
  402.3 36.1 %conditional.3 = ((f32[4,1024]{1,0:T(4,128)S(1)}, f32[4,1024]{1,0:T(4,128)S(1)}, f32[4,1024,64]{1,2,0:T(8,128)})) conditional(s32[]{:T(128)} %convert_element_type.106, (f32[4,1024]{1,0:T(4,128)S(1)}, f32[4,1024]{1,0:T(4,128)S(1)}, f32[4,1024,64]{1,2,0:T(8,128)}) %tuple.62, (s32[]{:T(128)}, s32[]{:T(128)}, s32[]{:T(128)}, ...), branch_computations={%region_4.4_spmd, %region_5.7_spmd} | conditional | flops 1923098624 | bytes 107565224 | solution.py:115
  411.2 9.2 %fusion.40 = (f32[4,1024]{1,0:T(4,128)S(1)}, f32[4,1024,1024]{1,2,0:T(8,128)}) fusion(bf16[1024,4,32]{0,2,1:T(8,128)(2,1)S(1)} %get-tuple-element.258, bf16[8,1024,32]{1,2,0:T(8,128)(2,1)} %get-tuple-element.257, s32[]{:T(128)S(6)} %select_n.18, f32[4,1024,1024]{2,1,0:T(8,128)S(1)} %fusion.15, pred[1024,1024]{0,1:T(8,128)(4,1)} %broadcast_compare_fusion), kind=kOutput, calls=%fused_computation.67 | convolution fusion | flops 285208576 | bytes 34947076 | tf_op jit(solution)/shard_map/while/body/eval_jaxpr/cond/branch_1_fun/qhd,kd->hqk/dot_general | solution.py:96
  420.4 9.2 %fusion.5 = f32[4,1024]{1,0:T(4,128)S(1)} fusion(f32[4,1024,1024]{1,2,0:T(8,128)} %get-tuple-element.389, f32[4,1024]{1,0:T(4,128)S(1)} %max.5, pred[1024,1024]{0,1:T(8,128)(4,1)} %broadcast_compare_fusion), kind=kLoop, calls=%fused_computation.6 | loop fusion | flops 12578816 | bytes 17858560 | tf_op jit(solution)/shard_map/while/body/eval_jaxpr/cond/branch_1_fun/reduce_sum | solution.py:106
  439.5 36.1 %conditional.3 = ((f32[4,1024]{1,0:T(4,128)S(1)}, f32[4,1024]{1,0:T(4,128)S(1)}, f32[4,1024,64]{1,2,0:T(8,128)})) conditional(s32[]{:T(128)} %convert_element_type.106, (f32[4,1024]{1,0:T(4,128)S(1)}, f32[4,1024]{1,0:T(4,128)S(1)}, f32[4,1024,64]{1,2,0:T(8,128)}) %tuple.62, (s32[]{:T(128)}, s32[]{:T(128)}, s32[]{:T(128)}, ...), branch_computations={%region_4.4_spmd, %region_5.7_spmd} | conditional | flops 1923098624 | bytes 107565224 | solution.py:115
  448.4 9.2 %fusion.40 = (f32[4,1024]{1,0:T(4,128)S(1)}, f32[4,1024,1024]{1,2,0:T(8,128)}) fusion(bf16[1024,4,32]{0,2,1:T(8,128)(2,1)S(1)} %get-tuple-element.258, bf16[8,1024,32]{1,2,0:T(8,128)(2,1)} %get-tuple-element.257, s32[]{:T(128)S(6)} %select_n.18, f32[4,1024,1024]{2,1,0:T(8,128)S(1)} %fusion.15, pred[1024,1024]{0,1:T(8,128)(4,1)} %broadcast_compare_fusion), kind=kOutput, calls=%fused_computation.67 | convolution fusion | flops 285208576 | bytes 34947076 | tf_op jit(solution)/shard_map/while/body/eval_jaxpr/cond/branch_1_fun/qhd,kd->hqk/dot_general | solution.py:96
  457.6 9.2 %fusion.5 = f32[4,1024]{1,0:T(4,128)S(1)} fusion(f32[4,1024,1024]{1,2,0:T(8,128)} %get-tuple-element.389, f32[4,1024]{1,0:T(4,128)S(1)} %max.5, pred[1024,1024]{0,1:T(8,128)(4,1)} %broadcast_compare_fusion), kind=kLoop, calls=%fused_computation.6 | loop fusion | flops 12578816 | bytes 17858560 | tf_op jit(solution)/shard_map/while/body/eval_jaxpr/cond/branch_1_fun/reduce_sum | solution.py:106
  477.4 11.4 %all_to_all.16 = bf16[4,256,256]{1,2,0:T(8,128)(2,1)S(1)} all-to-all(bf16[4,256,256]{1,2,0:T(8,128)(2,1)S(1)} %copy.21), channel_id=1, replica_groups=mesh['sp'=8,'tp'=4] {'tp'}, dimensions={0} | all-to-all | bytes 1048576 | tf_op jit(solution)/shard_map/all_to_all | solution.py:139
  (179 shorter events, 139.6 us)
Async XLA Ops:
  6.5 65.0 %copy-start = (bf16[768,384]{1,0:T(8,128)(2,1)S(1)}, bf16[768,384]{1,0:T(8,128)(2,1)}, u32[]{:S(2)}) copy-start(bf16[768,384]{1,0:T(8,128)(2,1)} %param.22) | copy-start | bytes 1769476
  6.5 25.2 %all-gather.4.cloned.1.call-start = ((), (), s32[]{:S(2)}) async-start(), calls=%async_computation.1 | async-start | bytes 1310720 | tf_op jit(solution)/shard_map/all_gather | solution.py:65
  8.7 4.4 copy-start.8
  8.7 5.3 %copy-start.5 = (bf16[256,4096]{1,0:T(8,128)(2,1)S(1)}, bf16[256,4096]{1,0:T(8,128)(2,1)}, u32[]{:S(2)}) copy-start(bf16[256,4096]{1,0:T(8,128)(2,1)} %param.15) | copy-start | bytes 6291460
  8.7 5.3 %copy-start.10 = (f32[4096]{0:T(1024)S(1)}, f32[4096]{0:T(1024)}, u32[]{:S(2)}) copy-start(f32[4096]{0:T(1024)} %param.16) | copy-start | bytes 49156
  14.0 4.8 copy-start.7
  14.0 17.9 %copy-start.9 = (bf16[4096,32]{0,1:T(8,128)(2,1)S(1)}, bf16[4096,32]{0,1:T(8,128)(2,1)}, u32[]{:S(2)}) copy-start(bf16[4096,32]{0,1:T(8,128)(2,1)} %param.19) | copy-start | bytes 786436
  14.0 57.5 %all-gather.8.cloned.1.call-start = ((), (), s32[]{:S(2)}) async-start(), calls=%async_computation.3 | async-start | bytes 1966080 | tf_op jit(solution)/shard_map/all_gather | solution.py:64
  19.7 157.1 %all-gather.6.cloned.1.call-start = ((), (), s32[]{:S(2)}) async-start(), calls=%async_computation.2 | async-start | bytes 9437184 | tf_op jit(solution)/shard_map/all_gather | solution.py:124
  184.6 1.0 copy-start.3
  197.1 9.2 %copy-start.2 = (pred[1024,1024]{0,1:T(8,128)(4,1)S(1)}, pred[1024,1024]{0,1:T(8,128)(4,1)}, u32[]{:S(2)}) copy-start(pred[1024,1024]{0,1:T(8,128)(4,1)} %broadcast_compare_fusion) | copy-start | bytes 3145732 | tf_op jit(solution)/shard_map/while/body/eval_jaxpr/cond
  197.1 9.2 %copy-start.4 = (bf16[1024,512]{0,1:T(8,128)(2,1)S(1)}, bf16[1024,512]{0,1:T(8,128)(2,1)}, u32[]{:S(2)}) copy-start(bf16[1024,512]{0,1:T(8,128)(2,1)} %copy-done.3) | copy-start | bytes 3145732 | tf_op jit(solution)/shard_map/while/body/eval_jaxpr/cond
  221.8 1.0 copy-start.3
  234.3 9.2 %copy-start.2 = (pred[1024,1024]{0,1:T(8,128)(4,1)S(1)}, pred[1024,1024]{0,1:T(8,128)(4,1)}, u32[]{:S(2)}) copy-start(pred[1024,1024]{0,1:T(8,128)(4,1)} %broadcast_compare_fusion) | copy-start | bytes 3145732 | tf_op jit(solution)/shard_map/while/body/eval_jaxpr/cond
  234.3 9.2 %copy-start.4 = (bf16[1024,512]{0,1:T(8,128)(2,1)S(1)}, bf16[1024,512]{0,1:T(8,128)(2,1)}, u32[]{:S(2)}) copy-start(bf16[1024,512]{0,1:T(8,128)(2,1)} %copy-done.3) | copy-start | bytes 3145732 | tf_op jit(solution)/shard_map/while/body/eval_jaxpr/cond
  259.0 1.0 copy-start.3
  271.5 9.2 %copy-start.2 = (pred[1024,1024]{0,1:T(8,128)(4,1)S(1)}, pred[1024,1024]{0,1:T(8,128)(4,1)}, u32[]{:S(2)}) copy-start(pred[1024,1024]{0,1:T(8,128)(4,1)} %broadcast_compare_fusion) | copy-start | bytes 3145732 | tf_op jit(solution)/shard_map/while/body/eval_jaxpr/cond
  271.5 9.2 %copy-start.4 = (bf16[1024,512]{0,1:T(8,128)(2,1)S(1)}, bf16[1024,512]{0,1:T(8,128)(2,1)}, u32[]{:S(2)}) copy-start(bf16[1024,512]{0,1:T(8,128)(2,1)} %copy-done.3) | copy-start | bytes 3145732 | tf_op jit(solution)/shard_map/while/body/eval_jaxpr/cond
  308.7 9.2 %copy-start.2 = (pred[1024,1024]{0,1:T(8,128)(4,1)S(1)}, pred[1024,1024]{0,1:T(8,128)(4,1)}, u32[]{:S(2)}) copy-start(pred[1024,1024]{0,1:T(8,128)(4,1)} %broadcast_compare_fusion) | copy-start | bytes 3145732 | tf_op jit(solution)/shard_map/while/body/eval_jaxpr/cond
  308.8 9.2 %copy-start.4 = (bf16[1024,512]{0,1:T(8,128)(2,1)S(1)}, bf16[1024,512]{0,1:T(8,128)(2,1)}, u32[]{:S(2)}) copy-start(bf16[1024,512]{0,1:T(8,128)(2,1)} %copy-done.3) | copy-start | bytes 3145732 | tf_op jit(solution)/shard_map/while/body/eval_jaxpr/cond
  333.4 1.0 copy-start.3
  346.0 9.2 %copy-start.2 = (pred[1024,1024]{0,1:T(8,128)(4,1)S(1)}, pred[1024,1024]{0,1:T(8,128)(4,1)}, u32[]{:S(2)}) copy-start(pred[1024,1024]{0,1:T(8,128)(4,1)} %broadcast_compare_fusion) | copy-start | bytes 3145732 | tf_op jit(solution)/shard_map/while/body/eval_jaxpr/cond
  346.0 9.2 %copy-start.4 = (bf16[1024,512]{0,1:T(8,128)(2,1)S(1)}, bf16[1024,512]{0,1:T(8,128)(2,1)}, u32[]{:S(2)}) copy-start(bf16[1024,512]{0,1:T(8,128)(2,1)} %copy-done.3) | copy-start | bytes 3145732 | tf_op jit(solution)/shard_map/while/body/eval_jaxpr/cond
  383.2 9.2 %copy-start.2 = (pred[1024,1024]{0,1:T(8,128)(4,1)S(1)}, pred[1024,1024]{0,1:T(8,128)(4,1)}, u32[]{:S(2)}) copy-start(pred[1024,1024]{0,1:T(8,128)(4,1)} %broadcast_compare_fusion) | copy-start | bytes 3145732 | tf_op jit(solution)/shard_map/while/body/eval_jaxpr/cond
  383.2 9.2 %copy-start.4 = (bf16[1024,512]{0,1:T(8,128)(2,1)S(1)}, bf16[1024,512]{0,1:T(8,128)(2,1)}, u32[]{:S(2)}) copy-start(bf16[1024,512]{0,1:T(8,128)(2,1)} %copy-done.3) | copy-start | bytes 3145732 | tf_op jit(solution)/shard_map/while/body/eval_jaxpr/cond
  407.9 1.0 copy-start.3
  420.4 9.2 %copy-start.2 = (pred[1024,1024]{0,1:T(8,128)(4,1)S(1)}, pred[1024,1024]{0,1:T(8,128)(4,1)}, u32[]{:S(2)}) copy-start(pred[1024,1024]{0,1:T(8,128)(4,1)} %broadcast_compare_fusion) | copy-start | bytes 3145732 | tf_op jit(solution)/shard_map/while/body/eval_jaxpr/cond
  420.4 9.2 %copy-start.4 = (bf16[1024,512]{0,1:T(8,128)(2,1)S(1)}, bf16[1024,512]{0,1:T(8,128)(2,1)}, u32[]{:S(2)}) copy-start(bf16[1024,512]{0,1:T(8,128)(2,1)} %copy-done.3) | copy-start | bytes 3145732 | tf_op jit(solution)/shard_map/while/body/eval_jaxpr/cond
  457.6 9.2 %copy-start.2 = (pred[1024,1024]{0,1:T(8,128)(4,1)S(1)}, pred[1024,1024]{0,1:T(8,128)(4,1)}, u32[]{:S(2)}) copy-start(pred[1024,1024]{0,1:T(8,128)(4,1)} %broadcast_compare_fusion) | copy-start | bytes 3145732 | tf_op jit(solution)/shard_map/while/body/eval_jaxpr/cond
  457.6 9.2 %copy-start.4 = (bf16[1024,512]{0,1:T(8,128)(2,1)S(1)}, bf16[1024,512]{0,1:T(8,128)(2,1)}, u32[]{:S(2)}) copy-start(bf16[1024,512]{0,1:T(8,128)(2,1)} %copy-done.3) | copy-start | bytes 3145732 | tf_op jit(solution)/shard_map/while/body/eval_jaxpr/cond
  488.7 6.0 %copy-start.6 = (f32[4096]{0:T(1024)S(1)}, f32[4096]{0:T(1024)}, u32[]{:S(2)}) copy-start(f32[4096]{0:T(1024)} %param.25) | copy-start | bytes 49156
  488.7 7.9 %copy-start.1 = (bf16[768,384]{1,0:T(8,128)(2,1)S(1)}, bf16[768,384]{1,0:T(8,128)(2,1)}, u32[]{:S(2)}) copy-start(bf16[768,384]{1,0:T(8,128)(2,1)} %param.22) | copy-start | bytes 1769476
  (3 other events, 2.9 us)
Sparse Core Ops, SparseCore 0:
  14.1 17.6 all-gather.3
  33.3 19.6 all-gather.7
  55.1 121.5 all-gather.5
where the time goes:
time: 504 us; the launch traced here: 503 us
  matrix products  197 us (39%)
  waiting for transfers between devices  115 us (23%)
  other arithmetic  94.9 us (19%)
  blocking collectives  48.9 us (10%)
  loops' own time  18.9 us (4%)
  local copies, waits for them, and re-layouts  14.8 us (3%)
  between operations  13.3 us (3%)
    all_gather x1, waiting for transfers between devices, local(): key_piece = lax.all_gather(kv_group, 'sp', axis=0, tiled=True)  103 us
    dot_general x8, matrix products, compute(): jnp.einsum('qhd,kd->hqk', query_rot, rot_rows, preferred_element_type=jnp...  73.2 us
    reduce_sum x8, other arithmetic, compute(): total_new = total * correction + jnp.sum(weights, axis=-1)  73.2 us
    dot_general x8, matrix products, compute(): jnp.einsum('hqk,khd->hqd', weights.astype(jnp.bfloat16), keys_values[...,...  70.1 us
    all_gather x1, blocking collectives, local(): rot_piece = lax.all_gather(rot_group, 'sp', axis=0, tiled=True)  32.3 us
    dot_general x8, matrix products, compute(): jnp.einsum('qhd,khd->hqk', query_nope, keys_values[..., :NOPE], preferred...  19 us
    dot_general x8, matrix products, compute(): jnp.dot(key_rows, kv_up, preferred_element_type=jnp.float32)  16.8 us
    another operation x8, loops' own time, attend_block(): lax.cond(block_first <= query_first + group_rows - 1, compute, lambda sta...  14.3 us
  transfers between devices with their start and end apart: 3, of which 2 were waited for; matrix products, arithmetic and copies ran while one was open for 2% of the time, Pallas kernels for 0%

commit v1 on v0

--- a/solution.py
+++ b/solution.py
@@ -121,8 +121,11 @@
         jnp.zeros((head_count, group_rows), jnp.float32),
         jnp.zeros((head_count, group_rows, VDIM), jnp.float32),
     )
-    key_piece = lax.all_gather(kv_group, "sp", axis=0, tiled=True)
-    rot_piece = lax.all_gather(rot_group, "sp", axis=0, tiled=True)
+    key_piece, rot_piece = jnp.split(
+        lax.all_gather(jnp.concatenate([kv_group, rot_group], 1), "sp", axis=0, tiled=True),
+        [kv_group.shape[1]],
+        1,
+    )
     piece_rows = rot_piece.shape[0]
     block_count = piece_rows // group_rows
     key_blocks = key_piece.reshape((block_count, group_rows) + key_piece.shape[1:])

time: 504 us -> 547 us (1.085)
  waiting for transfers between devices: 115 us -> 171 us
  blocking collectives: 48.9 us -> 18.7 us
  local copies, waits for them, and re-layouts: 14.8 us -> 25.2 us
    all_gather x1, waiting for transfers between devices: 103 us -> 147 us  [local(): lax.all_gather(jnp.concatenate([kv_group, rot_group], 1), 'sp', axis=0, t...]
    all_gather x1 -> x0, blocking collectives: 32.3 us -> none  [local(): rot_piece = lax.all_gather(rot_group, 'sp', axis=0, tiled=True)]
    all_gather x1, waiting for transfers between devices: 0.02 us -> 18.8 us  [local(): lax.all_gather(q_lat, 'tp', axis=0, tiled=True)]
    split x0 -> x3, local copies, waits for them, and re-layouts: none -> 8.74 us  [local(): jnp.split(lax.all_gather(jnp.concatenate([kv_group, rot_group], 1), 'sp',...]
    all_gather x1, waiting for transfers between devices: 12 us -> 4.79 us  [local(): lax.all_gather(kv_lat, 'tp', axis=0, tiled=True)]
  transfers between devices with their start and end apart: 3 -> 3, of which waited for: 2 -> 3; matrix products, arithmetic and copies ran while one was open for 2% -> 2% of each run, Pallas kernels for 0% -> 0%
where the time goes in v1:
time: 547 us; the launch traced here: 546 us
  matrix products  197 us (36%)
  waiting for transfers between devices  171 us (31%)
  other arithmetic  97.2 us (18%)
  local copies, waits for them, and re-layouts  25.2 us (5%)
  loops' own time  22.9 us (4%)
  blocking collectives  18.7 us (3%)
  between operations  13.3 us (2%)
    all_gather x1, waiting for transfers between devices, local(): lax.all_gather(jnp.concatenate([kv_group, rot_group], 1), 'sp', axis=0, t...  147 us
    reduce_sum x8, other arithmetic, compute(): total_new = total * correction + jnp.sum(weights, axis=-1)  73.2 us
    dot_general x8, matrix products, compute(): jnp.einsum('qhd,kd->hqk', query_rot, rot_rows, preferred_element_type=jnp...  73.2 us
    dot_general x8, matrix products, compute(): jnp.einsum('hqk,khd->hqd', weights.astype(jnp.bfloat16), keys_values[...,...  70 us
    dot_general x8, matrix products, compute(): jnp.einsum('qhd,khd->hqk', query_nope, keys_values[..., :NOPE], preferred...  19 us
    all_gather x1, waiting for transfers between devices, local(): lax.all_gather(q_lat, 'tp', axis=0, tiled=True)  18.8 us
    another operation x8, loops' own time, attend_block(): lax.cond(block_first <= query_first + group_rows - 1, compute, lambda sta...  17.2 us
    dot_general x8, matrix products, compute(): jnp.dot(key_rows, kv_up, preferred_element_type=jnp.float32)  16.8 us
  transfers between devices with their start and end apart: 3, of which 3 were waited for; matrix products, arithmetic and copies ran while one was open for 2% of the time, Pallas kernels for 0%

profile of v1, /device:TPU:26, one launch (start us, length us, event | category | flops | bytes accessed | tf_op | source)
XLA Modules:
  0.0 545.6 jit_solution(12571945991478774259)
XLA Ops:
  35.7 18.8 %all-gather.8.cloned.1.call-done = bf16[1024,768]{1,0:T(8,128)(2,1)} async-done(((bf16[256,768]{1,0:T(8,128)(2,1)}), bf16[1024,768]{1,0:T(8,128)(2,1)}) %all-gather.8.cloned.1.call-update) | async-done | bytes 1572880 | tf_op jit(solution)/shard_map/all_gather | solution.py:64
  56.8 147.5 %all-gather.6.cloned.1.call-done = bf16[8192,544]{1,0:T(8,128)(2,1)} async-done(((bf16[1024,544]{1,0:T(8,128)(2,1)}), bf16[8192,544]{1,0:T(8,128)(2,1)}) %all-gather.6.cloned.1.call-update) | async-done | bytes 8912912 | tf_op jit(solution)/shard_map/all_gather | solution.py:125
  215.7 302.4 %while.17 = (s32[]{:T(128)}, f32[4,1024]{1,0:T(4,128)S(1)}, f32[4,1024]{1,0:T(4,128)S(1)}, f32[4,1024,64]{1,2,0:T(8,128)}, s32[8]{0:T(128)S(1)}, /*index=5*/s32[...) while((s32[]{:T(128)}, f32[4,1024]{1,0:T(4,128)S(1)}, ...), condition=%wide.region_8.9_spmd.clone, body=%wide.region_3.8_spmd.clone.sunk | while | flops 1923098624 | bytes 107569616 | solution.py:138
  217.0 36.4 %conditional.3 = ((f32[4,1024]{1,0:T(4,128)S(1)}, f32[4,1024]{1,0:T(4,128)S(1)}, f32[4,1024,64]{1,2,0:T(8,128)})) conditional(s32[]{:T(128)} %convert_element_type.106, (f32[4,1024]{1,0:T(4,128)S(1)}, f32[4,1024]{1,0:T(4,128)S(1)}, f32[4,1024,64]{1,2,0:T(8,128)}) %tuple.62, (s32[]{:T(128)}, s32[]{:T(128)}, s32[]{:T(128)}, ...), branch_computations={%region_4.4_spmd, %region_5.7_spmd} | conditional | flops 1923098624 | bytes 107565224 | solution.py:115
  226.3 9.2 %fusion.40 = (f32[4,1024]{1,0:T(4,128)S(1)}, f32[4,1024,1024]{1,2,0:T(8,128)}) fusion(bf16[1024,4,32]{0,2,1:T(8,128)(2,1)S(1)} %get-tuple-element.258, bf16[8,1024,32]{1,2,0:T(8,128)(2,1)} %get-tuple-element.257, s32[]{:T(128)S(6)} %select_n.18, f32[4,1024,1024]{2,1,0:T(8,128)S(1)} %fusion.15, pred[1024,1024]{0,1:T(8,128)(4,1)} %broadcast_compare_fusion), kind=kOutput, calls=%fused_computation.67 | convolution fusion | flops 285208576 | bytes 34947076 | tf_op jit(solution)/shard_map/while/body/eval_jaxpr/cond/branch_1_fun/qhd,kd->hqk/dot_general | solution.py:96
  235.5 9.2 %fusion.5 = f32[4,1024]{1,0:T(4,128)S(1)} fusion(f32[4,1024,1024]{1,2,0:T(8,128)} %get-tuple-element.389, f32[4,1024]{1,0:T(4,128)S(1)} %max.5, pred[1024,1024]{0,1:T(8,128)(4,1)} %broadcast_compare_fusion), kind=kLoop, calls=%fused_computation.6 | loop fusion | flops 12578816 | bytes 17858560 | tf_op jit(solution)/shard_map/while/body/eval_jaxpr/cond/branch_1_fun/reduce_sum | solution.py:106
  244.7 8.8 %fusion.9 = f32[4,1024,64]{1,2,0:T(8,128)} fusion(f32[4,1024,1024]{1,2,0:T(8,128)} %get-tuple-element.389, f32[4,1024]{1,0:T(4,128)S(1)} %max.5, pred[1024,1024]{0,1:T(8,128)(4,1)S(1)} %copy-done.2, f32[4,1024,64]{1,2,0:T(8,128)} %get-tuple-element.260, bf16[1024,4,128]{0,2,1:T(8,128)(2,1)S(1)} %bitcast.42, f32[4,1024]{1,0:T(4,128)S(1)} %get-tuple-element.387), kind=kOutput, calls=%fused_computation.11 | convolution fusion | flops 549978112 | bytes 20480000 | tf_op jit(solution)/shard_map/while/body/eval_jaxpr/cond/branch_1_fun/hqk,khd->hqd/dot_general | solution.py:107
  254.8 36.4 %conditional.3 = ((f32[4,1024]{1,0:T(4,128)S(1)}, f32[4,1024]{1,0:T(4,128)S(1)}, f32[4,1024,64]{1,2,0:T(8,128)})) conditional(s32[]{:T(128)} %convert_element_type.106, (f32[4,1024]{1,0:T(4,128)S(1)}, f32[4,1024]{1,0:T(4,128)S(1)}, f32[4,1024,64]{1,2,0:T(8,128)}) %tuple.62, (s32[]{:T(128)}, s32[]{:T(128)}, s32[]{:T(128)}, ...), branch_computations={%region_4.4_spmd, %region_5.7_spmd} | conditional | flops 1923098624 | bytes 107565224 | solution.py:115
  264.1 9.2 %fusion.40 = (f32[4,1024]{1,0:T(4,128)S(1)}, f32[4,1024,1024]{1,2,0:T(8,128)}) fusion(bf16[1024,4,32]{0,2,1:T(8,128)(2,1)S(1)} %get-tuple-element.258, bf16[8,1024,32]{1,2,0:T(8,128)(2,1)} %get-tuple-element.257, s32[]{:T(128)S(6)} %select_n.18, f32[4,1024,1024]{2,1,0:T(8,128)S(1)} %fusion.15, pred[1024,1024]{0,1:T(8,128)(4,1)} %broadcast_compare_fusion), kind=kOutput, calls=%fused_computation.67 | convolution fusion | flops 285208576 | bytes 34947076 | tf_op jit(solution)/shard_map/while/body/eval_jaxpr/cond/branch_1_fun/qhd,kd->hqk/dot_general | solution.py:96
  273.3 9.2 %fusion.5 = f32[4,1024]{1,0:T(4,128)S(1)} fusion(f32[4,1024,1024]{1,2,0:T(8,128)} %get-tuple-element.389, f32[4,1024]{1,0:T(4,128)S(1)} %max.5, pred[1024,1024]{0,1:T(8,128)(4,1)} %broadcast_compare_fusion), kind=kLoop, calls=%fused_computation.6 | loop fusion | flops 12578816 | bytes 17858560 | tf_op jit(solution)/shard_map/while/body/eval_jaxpr/cond/branch_1_fun/reduce_sum | solution.py:106
  282.5 8.8 %fusion.9 = f32[4,1024,64]{1,2,0:T(8,128)} fusion(f32[4,1024,1024]{1,2,0:T(8,128)} %get-tuple-element.389, f32[4,1024]{1,0:T(4,128)S(1)} %max.5, pred[1024,1024]{0,1:T(8,128)(4,1)S(1)} %copy-done.2, f32[4,1024,64]{1,2,0:T(8,128)} %get-tuple-element.260, bf16[1024,4,128]{0,2,1:T(8,128)(2,1)S(1)} %bitcast.42, f32[4,1024]{1,0:T(4,128)S(1)} %get-tuple-element.387), kind=kOutput, calls=%fused_computation.11 | convolution fusion | flops 549978112 | bytes 20480000 | tf_op jit(solution)/shard_map/while/body/eval_jaxpr/cond/branch_1_fun/hqk,khd->hqd/dot_general | solution.py:107
  292.6 36.4 %conditional.3 = ((f32[4,1024]{1,0:T(4,128)S(1)}, f32[4,1024]{1,0:T(4,128)S(1)}, f32[4,1024,64]{1,2,0:T(8,128)})) conditional(s32[]{:T(128)} %convert_element_type.106, (f32[4,1024]{1,0:T(4,128)S(1)}, f32[4,1024]{1,0:T(4,128)S(1)}, f32[4,1024,64]{1,2,0:T(8,128)}) %tuple.62, (s32[]{:T(128)}, s32[]{:T(128)}, s32[]{:T(128)}, ...), branch_computations={%region_4.4_spmd, %region_5.7_spmd} | conditional | flops 1923098624 | bytes 107565224 | solution.py:115
  301.9 9.2 %fusion.40 = (f32[4,1024]{1,0:T(4,128)S(1)}, f32[4,1024,1024]{1,2,0:T(8,128)}) fusion(bf16[1024,4,32]{0,2,1:T(8,128)(2,1)S(1)} %get-tuple-element.258, bf16[8,1024,32]{1,2,0:T(8,128)(2,1)} %get-tuple-element.257, s32[]{:T(128)S(6)} %select_n.18, f32[4,1024,1024]{2,1,0:T(8,128)S(1)} %fusion.15, pred[1024,1024]{0,1:T(8,128)(4,1)} %broadcast_compare_fusion), kind=kOutput, calls=%fused_computation.67 | convolution fusion | flops 285208576 | bytes 34947076 | tf_op jit(solution)/shard_map/while/body/eval_jaxpr/cond/branch_1_fun/qhd,kd->hqk/dot_general | solution.py:96
  311.1 9.2 %fusion.5 = f32[4,1024]{1,0:T(4,128)S(1)} fusion(f32[4,1024,1024]{1,2,0:T(8,128)} %get-tuple-element.389, f32[4,1024]{1,0:T(4,128)S(1)} %max.5, pred[1024,1024]{0,1:T(8,128)(4,1)} %broadcast_compare_fusion), kind=kLoop, calls=%fused_computation.6 | loop fusion | flops 12578816 | bytes 17858560 | tf_op jit(solution)/shard_map/while/body/eval_jaxpr/cond/branch_1_fun/reduce_sum | solution.py:106
  330.4 36.4 %conditional.3 = ((f32[4,1024]{1,0:T(4,128)S(1)}, f32[4,1024]{1,0:T(4,128)S(1)}, f32[4,1024,64]{1,2,0:T(8,128)})) conditional(s32[]{:T(128)} %convert_element_type.106, (f32[4,1024]{1,0:T(4,128)S(1)}, f32[4,1024]{1,0:T(4,128)S(1)}, f32[4,1024,64]{1,2,0:T(8,128)}) %tuple.62, (s32[]{:T(128)}, s32[]{:T(128)}, s32[]{:T(128)}, ...), branch_computations={%region_4.4_spmd, %region_5.7_spmd} | conditional | flops 1923098624 | bytes 107565224 | solution.py:115
  339.7 9.2 %fusion.40 = (f32[4,1024]{1,0:T(4,128)S(1)}, f32[4,1024,1024]{1,2,0:T(8,128)}) fusion(bf16[1024,4,32]{0,2,1:T(8,128)(2,1)S(1)} %get-tuple-element.258, bf16[8,1024,32]{1,2,0:T(8,128)(2,1)} %get-tuple-element.257, s32[]{:T(128)S(6)} %select_n.18, f32[4,1024,1024]{2,1,0:T(8,128)S(1)} %fusion.15, pred[1024,1024]{0,1:T(8,128)(4,1)} %broadcast_compare_fusion), kind=kOutput, calls=%fused_computation.67 | convolution fusion | flops 285208576 | bytes 34947076 | tf_op jit(solution)/shard_map/while/body/eval_jaxpr/cond/branch_1_fun/qhd,kd->hqk/dot_general | solution.py:96
  348.9 9.2 %fusion.5 = f32[4,1024]{1,0:T(4,128)S(1)} fusion(f32[4,1024,1024]{1,2,0:T(8,128)} %get-tuple-element.389, f32[4,1024]{1,0:T(4,128)S(1)} %max.5, pred[1024,1024]{0,1:T(8,128)(4,1)} %broadcast_compare_fusion), kind=kLoop, calls=%fused_computation.6 | loop fusion | flops 12578816 | bytes 17858560 | tf_op jit(solution)/shard_map/while/body/eval_jaxpr/cond/branch_1_fun/reduce_sum | solution.py:106
  368.2 36.4 %conditional.3 = ((f32[4,1024]{1,0:T(4,128)S(1)}, f32[4,1024]{1,0:T(4,128)S(1)}, f32[4,1024,64]{1,2,0:T(8,128)})) conditional(s32[]{:T(128)} %convert_element_type.106, (f32[4,1024]{1,0:T(4,128)S(1)}, f32[4,1024]{1,0:T(4,128)S(1)}, f32[4,1024,64]{1,2,0:T(8,128)}) %tuple.62, (s32[]{:T(128)}, s32[]{:T(128)}, s32[]{:T(128)}, ...), branch_computations={%region_4.4_spmd, %region_5.7_spmd} | conditional | flops 1923098624 | bytes 107565224 | solution.py:115
  377.5 9.2 %fusion.40 = (f32[4,1024]{1,0:T(4,128)S(1)}, f32[4,1024,1024]{1,2,0:T(8,128)}) fusion(bf16[1024,4,32]{0,2,1:T(8,128)(2,1)S(1)} %get-tuple-element.258, bf16[8,1024,32]{1,2,0:T(8,128)(2,1)} %get-tuple-element.257, s32[]{:T(128)S(6)} %select_n.18, f32[4,1024,1024]{2,1,0:T(8,128)S(1)} %fusion.15, pred[1024,1024]{0,1:T(8,128)(4,1)} %broadcast_compare_fusion), kind=kOutput, calls=%fused_computation.67 | convolution fusion | flops 285208576 | bytes 34947076 | tf_op jit(solution)/shard_map/while/body/eval_jaxpr/cond/branch_1_fun/qhd,kd->hqk/dot_general | solution.py:96
  386.7 9.2 %fusion.5 = f32[4,1024]{1,0:T(4,128)S(1)} fusion(f32[4,1024,1024]{1,2,0:T(8,128)} %get-tuple-element.389, f32[4,1024]{1,0:T(4,128)S(1)} %max.5, pred[1024,1024]{0,1:T(8,128)(4,1)} %broadcast_compare_fusion), kind=kLoop, calls=%fused_computation.6 | loop fusion | flops 12578816 | bytes 17858560 | tf_op jit(solution)/shard_map/while/body/eval_jaxpr/cond/branch_1_fun/reduce_sum | solution.py:106
  395.9 8.8 %fusion.9 = f32[4,1024,64]{1,2,0:T(8,128)} fusion(f32[4,1024,1024]{1,2,0:T(8,128)} %get-tuple-element.389, f32[4,1024]{1,0:T(4,128)S(1)} %max.5, pred[1024,1024]{0,1:T(8,128)(4,1)S(1)} %copy-done.2, f32[4,1024,64]{1,2,0:T(8,128)} %get-tuple-element.260, bf16[1024,4,128]{0,2,1:T(8,128)(2,1)S(1)} %bitcast.42, f32[4,1024]{1,0:T(4,128)S(1)} %get-tuple-element.387), kind=kOutput, calls=%fused_computation.11 | convolution fusion | flops 549978112 | bytes 20480000 | tf_op jit(solution)/shard_map/while/body/eval_jaxpr/cond/branch_1_fun/hqk,khd->hqd/dot_general | solution.py:107
  406.0 36.4 %conditional.3 = ((f32[4,1024]{1,0:T(4,128)S(1)}, f32[4,1024]{1,0:T(4,128)S(1)}, f32[4,1024,64]{1,2,0:T(8,128)})) conditional(s32[]{:T(128)} %convert_element_type.106, (f32[4,1024]{1,0:T(4,128)S(1)}, f32[4,1024]{1,0:T(4,128)S(1)}, f32[4,1024,64]{1,2,0:T(8,128)}) %tuple.62, (s32[]{:T(128)}, s32[]{:T(128)}, s32[]{:T(128)}, ...), branch_computations={%region_4.4_spmd, %region_5.7_spmd} | conditional | flops 1923098624 | bytes 107565224 | solution.py:115
  415.3 9.2 %fusion.40 = (f32[4,1024]{1,0:T(4,128)S(1)}, f32[4,1024,1024]{1,2,0:T(8,128)}) fusion(bf16[1024,4,32]{0,2,1:T(8,128)(2,1)S(1)} %get-tuple-element.258, bf16[8,1024,32]{1,2,0:T(8,128)(2,1)} %get-tuple-element.257, s32[]{:T(128)S(6)} %select_n.18, f32[4,1024,1024]{2,1,0:T(8,128)S(1)} %fusion.15, pred[1024,1024]{0,1:T(8,128)(4,1)} %broadcast_compare_fusion), kind=kOutput, calls=%fused_computation.67 | convolution fusion | flops 285208576 | bytes 34947076 | tf_op jit(solution)/shard_map/while/body/eval_jaxpr/cond/branch_1_fun/qhd,kd->hqk/dot_general | solution.py:96
  424.5 9.2 %fusion.5 = f32[4,1024]{1,0:T(4,128)S(1)} fusion(f32[4,1024,1024]{1,2,0:T(8,128)} %get-tuple-element.389, f32[4,1024]{1,0:T(4,128)S(1)} %max.5, pred[1024,1024]{0,1:T(8,128)(4,1)} %broadcast_compare_fusion), kind=kLoop, calls=%fused_computation.6 | loop fusion | flops 12578816 | bytes 17858560 | tf_op jit(solution)/shard_map/while/body/eval_jaxpr/cond/branch_1_fun/reduce_sum | solution.py:106
  433.7 8.8 %fusion.9 = f32[4,1024,64]{1,2,0:T(8,128)} fusion(f32[4,1024,1024]{1,2,0:T(8,128)} %get-tuple-element.389, f32[4,1024]{1,0:T(4,128)S(1)} %max.5, pred[1024,1024]{0,1:T(8,128)(4,1)S(1)} %copy-done.2, f32[4,1024,64]{1,2,0:T(8,128)} %get-tuple-element.260, bf16[1024,4,128]{0,2,1:T(8,128)(2,1)S(1)} %bitcast.42, f32[4,1024]{1,0:T(4,128)S(1)} %get-tuple-element.387), kind=kOutput, calls=%fused_computation.11 | convolution fusion | flops 549978112 | bytes 20480000 | tf_op jit(solution)/shard_map/while/body/eval_jaxpr/cond/branch_1_fun/hqk,khd->hqd/dot_general | solution.py:107
  443.8 36.4 %conditional.3 = ((f32[4,1024]{1,0:T(4,128)S(1)}, f32[4,1024]{1,0:T(4,128)S(1)}, f32[4,1024,64]{1,2,0:T(8,128)})) conditional(s32[]{:T(128)} %convert_element_type.106, (f32[4,1024]{1,0:T(4,128)S(1)}, f32[4,1024]{1,0:T(4,128)S(1)}, f32[4,1024,64]{1,2,0:T(8,128)}) %tuple.62, (s32[]{:T(128)}, s32[]{:T(128)}, s32[]{:T(128)}, ...), branch_computations={%region_4.4_spmd, %region_5.7_spmd} | conditional | flops 1923098624 | bytes 107565224 | solution.py:115
  453.1 9.2 %fusion.40 = (f32[4,1024]{1,0:T(4,128)S(1)}, f32[4,1024,1024]{1,2,0:T(8,128)}) fusion(bf16[1024,4,32]{0,2,1:T(8,128)(2,1)S(1)} %get-tuple-element.258, bf16[8,1024,32]{1,2,0:T(8,128)(2,1)} %get-tuple-element.257, s32[]{:T(128)S(6)} %select_n.18, f32[4,1024,1024]{2,1,0:T(8,128)S(1)} %fusion.15, pred[1024,1024]{0,1:T(8,128)(4,1)} %broadcast_compare_fusion), kind=kOutput, calls=%fused_computation.67 | convolution fusion | flops 285208576 | bytes 34947076 | tf_op jit(solution)/shard_map/while/body/eval_jaxpr/cond/branch_1_fun/qhd,kd->hqk/dot_general | solution.py:96
  462.3 9.2 %fusion.5 = f32[4,1024]{1,0:T(4,128)S(1)} fusion(f32[4,1024,1024]{1,2,0:T(8,128)} %get-tuple-element.389, f32[4,1024]{1,0:T(4,128)S(1)} %max.5, pred[1024,1024]{0,1:T(8,128)(4,1)} %broadcast_compare_fusion), kind=kLoop, calls=%fused_computation.6 | loop fusion | flops 12578816 | bytes 17858560 | tf_op jit(solution)/shard_map/while/body/eval_jaxpr/cond/branch_1_fun/reduce_sum | solution.py:106
  481.6 36.4 %conditional.3 = ((f32[4,1024]{1,0:T(4,128)S(1)}, f32[4,1024]{1,0:T(4,128)S(1)}, f32[4,1024,64]{1,2,0:T(8,128)})) conditional(s32[]{:T(128)} %convert_element_type.106, (f32[4,1024]{1,0:T(4,128)S(1)}, f32[4,1024]{1,0:T(4,128)S(1)}, f32[4,1024,64]{1,2,0:T(8,128)}) %tuple.62, (s32[]{:T(128)}, s32[]{:T(128)}, s32[]{:T(128)}, ...), branch_computations={%region_4.4_spmd, %region_5.7_spmd} | conditional | flops 1923098624 | bytes 107565224 | solution.py:115
  490.9 9.2 %fusion.40 = (f32[4,1024]{1,0:T(4,128)S(1)}, f32[4,1024,1024]{1,2,0:T(8,128)}) fusion(bf16[1024,4,32]{0,2,1:T(8,128)(2,1)S(1)} %get-tuple-element.258, bf16[8,1024,32]{1,2,0:T(8,128)(2,1)} %get-tuple-element.257, s32[]{:T(128)S(6)} %select_n.18, f32[4,1024,1024]{2,1,0:T(8,128)S(1)} %fusion.15, pred[1024,1024]{0,1:T(8,128)(4,1)} %broadcast_compare_fusion), kind=kOutput, calls=%fused_computation.67 | convolution fusion | flops 285208576 | bytes 34947076 | tf_op jit(solution)/shard_map/while/body/eval_jaxpr/cond/branch_1_fun/qhd,kd->hqk/dot_general | solution.py:96
  500.1 9.2 %fusion.5 = f32[4,1024]{1,0:T(4,128)S(1)} fusion(f32[4,1024,1024]{1,2,0:T(8,128)} %get-tuple-element.389, f32[4,1024]{1,0:T(4,128)S(1)} %max.5, pred[1024,1024]{0,1:T(8,128)(4,1)} %broadcast_compare_fusion), kind=kLoop, calls=%fused_computation.6 | loop fusion | flops 12578816 | bytes 17858560 | tf_op jit(solution)/shard_map/while/body/eval_jaxpr/cond/branch_1_fun/reduce_sum | solution.py:106
  519.8 11.4 %all_to_all.16 = bf16[4,256,256]{1,2,0:T(8,128)(2,1)S(1)} all-to-all(bf16[4,256,256]{1,2,0:T(8,128)(2,1)S(1)} %copy.28), channel_id=1, replica_groups=mesh['sp'=8,'tp'=4] {'tp'}, dimensions={0} | all-to-all | bytes 1048576 | tf_op jit(solution)/shard_map/all_to_all | solution.py:142
  (183 shorter events, 150.3 us)
Async XLA Ops:
  6.5 47.9 %copy-start = (bf16[768,384]{1,0:T(8,128)(2,1)S(1)}, bf16[768,384]{1,0:T(8,128)(2,1)}, u32[]{:S(2)}) copy-start(bf16[768,384]{1,0:T(8,128)(2,1)} %param.22) | copy-start | bytes 1769476
  6.5 26.4 %all-gather.4.cloned.1.call-start = ((), (), s32[]{:S(2)}) async-start(), calls=%async_computation.1 | async-start | bytes 1310720 | tf_op jit(solution)/shard_map/all_gather | solution.py:65
  8.7 4.4 copy-start.8
  8.7 5.3 copy-start.5
  8.7 5.3 copy-start.10
  13.9 4.8 copy-start.7
  14.0 5.8 %copy-start.9 = (bf16[4096,32]{0,1:T(8,128)(2,1)S(1)}, bf16[4096,32]{0,1:T(8,128)(2,1)}, u32[]{:S(2)}) copy-start(bf16[4096,32]{0,1:T(8,128)(2,1)} %param.19) | copy-start | bytes 786436
  14.0 40.4 %all-gather.8.cloned.1.call-start = ((), (), s32[]{:S(2)}) async-start(), calls=%async_computation.3 | async-start | bytes 1966080 | tf_op jit(solution)/shard_map/all_gather | solution.py:64
  19.7 184.6 %all-gather.6.cloned.1.call-start = ((), (), s32[]{:S(2)}) async-start(), calls=%async_computation.2 | async-start | bytes 11796480 | tf_op jit(solution)/shard_map/all_gather | solution.py:125
  204.3 1.6 slice-start
  235.5 9.2 %copy-start.2 = (pred[1024,1024]{0,1:T(8,128)(4,1)S(1)}, pred[1024,1024]{0,1:T(8,128)(4,1)}, u32[]{:S(2)}) copy-start(pred[1024,1024]{0,1:T(8,128)(4,1)} %broadcast_compare_fusion) | copy-start | bytes 3145732 | tf_op jit(solution)/shard_map/while/body/eval_jaxpr/cond
  235.5 9.2 %copy-start.4 = (bf16[1024,512]{0,1:T(8,128)(2,1)S(1)}, bf16[1024,512]{0,1:T(8,128)(2,1)}, u32[]{:S(2)}) copy-start(bf16[1024,512]{0,1:T(8,128)(2,1)} %copy-done.3) | copy-start | bytes 3145732 | tf_op jit(solution)/shard_map/while/body/eval_jaxpr/cond
  260.8 1.0 copy-start.3
  273.3 9.2 %copy-start.2 = (pred[1024,1024]{0,1:T(8,128)(4,1)S(1)}, pred[1024,1024]{0,1:T(8,128)(4,1)}, u32[]{:S(2)}) copy-start(pred[1024,1024]{0,1:T(8,128)(4,1)} %broadcast_compare_fusion) | copy-start | bytes 3145732 | tf_op jit(solution)/shard_map/while/body/eval_jaxpr/cond
  273.3 9.2 %copy-start.4 = (bf16[1024,512]{0,1:T(8,128)(2,1)S(1)}, bf16[1024,512]{0,1:T(8,128)(2,1)}, u32[]{:S(2)}) copy-start(bf16[1024,512]{0,1:T(8,128)(2,1)} %copy-done.3) | copy-start | bytes 3145732 | tf_op jit(solution)/shard_map/while/body/eval_jaxpr/cond
  298.5 1.0 copy-start.3
  311.1 9.2 %copy-start.2 = (pred[1024,1024]{0,1:T(8,128)(4,1)S(1)}, pred[1024,1024]{0,1:T(8,128)(4,1)}, u32[]{:S(2)}) copy-start(pred[1024,1024]{0,1:T(8,128)(4,1)} %broadcast_compare_fusion) | copy-start | bytes 3145732 | tf_op jit(solution)/shard_map/while/body/eval_jaxpr/cond
  311.1 9.2 %copy-start.4 = (bf16[1024,512]{0,1:T(8,128)(2,1)S(1)}, bf16[1024,512]{0,1:T(8,128)(2,1)}, u32[]{:S(2)}) copy-start(bf16[1024,512]{0,1:T(8,128)(2,1)} %copy-done.3) | copy-start | bytes 3145732 | tf_op jit(solution)/shard_map/while/body/eval_jaxpr/cond
  348.9 9.2 %copy-start.2 = (pred[1024,1024]{0,1:T(8,128)(4,1)S(1)}, pred[1024,1024]{0,1:T(8,128)(4,1)}, u32[]{:S(2)}) copy-start(pred[1024,1024]{0,1:T(8,128)(4,1)} %broadcast_compare_fusion) | copy-start | bytes 3145732 | tf_op jit(solution)/shard_map/while/body/eval_jaxpr/cond
  348.9 9.2 %copy-start.4 = (bf16[1024,512]{0,1:T(8,128)(2,1)S(1)}, bf16[1024,512]{0,1:T(8,128)(2,1)}, u32[]{:S(2)}) copy-start(bf16[1024,512]{0,1:T(8,128)(2,1)} %copy-done.3) | copy-start | bytes 3145732 | tf_op jit(solution)/shard_map/while/body/eval_jaxpr/cond
  386.7 9.2 %copy-start.2 = (pred[1024,1024]{0,1:T(8,128)(4,1)S(1)}, pred[1024,1024]{0,1:T(8,128)(4,1)}, u32[]{:S(2)}) copy-start(pred[1024,1024]{0,1:T(8,128)(4,1)} %broadcast_compare_fusion) | copy-start | bytes 3145732 | tf_op jit(solution)/shard_map/while/body/eval_jaxpr/cond
  386.7 9.2 %copy-start.4 = (bf16[1024,512]{0,1:T(8,128)(2,1)S(1)}, bf16[1024,512]{0,1:T(8,128)(2,1)}, u32[]{:S(2)}) copy-start(bf16[1024,512]{0,1:T(8,128)(2,1)} %copy-done.3) | copy-start | bytes 3145732 | tf_op jit(solution)/shard_map/while/body/eval_jaxpr/cond
  424.4 9.2 %copy-start.2 = (pred[1024,1024]{0,1:T(8,128)(4,1)S(1)}, pred[1024,1024]{0,1:T(8,128)(4,1)}, u32[]{:S(2)}) copy-start(pred[1024,1024]{0,1:T(8,128)(4,1)} %broadcast_compare_fusion) | copy-start | bytes 3145732 | tf_op jit(solution)/shard_map/while/body/eval_jaxpr/cond
  424.5 9.2 %copy-start.4 = (bf16[1024,512]{0,1:T(8,128)(2,1)S(1)}, bf16[1024,512]{0,1:T(8,128)(2,1)}, u32[]{:S(2)}) copy-start(bf16[1024,512]{0,1:T(8,128)(2,1)} %copy-done.3) | copy-start | bytes 3145732 | tf_op jit(solution)/shard_map/while/body/eval_jaxpr/cond
  449.7 1.0 copy-start.3
  462.2 9.2 %copy-start.2 = (pred[1024,1024]{0,1:T(8,128)(4,1)S(1)}, pred[1024,1024]{0,1:T(8,128)(4,1)}, u32[]{:S(2)}) copy-start(pred[1024,1024]{0,1:T(8,128)(4,1)} %broadcast_compare_fusion) | copy-start | bytes 3145732 | tf_op jit(solution)/shard_map/while/body/eval_jaxpr/cond
  462.2 9.2 %copy-start.4 = (bf16[1024,512]{0,1:T(8,128)(2,1)S(1)}, bf16[1024,512]{0,1:T(8,128)(2,1)}, u32[]{:S(2)}) copy-start(bf16[1024,512]{0,1:T(8,128)(2,1)} %copy-done.3) | copy-start | bytes 3145732 | tf_op jit(solution)/shard_map/while/body/eval_jaxpr/cond
  487.5 1.0 copy-start.3
  500.0 9.2 %copy-start.2 = (pred[1024,1024]{0,1:T(8,128)(4,1)S(1)}, pred[1024,1024]{0,1:T(8,128)(4,1)}, u32[]{:S(2)}) copy-start(pred[1024,1024]{0,1:T(8,128)(4,1)} %broadcast_compare_fusion) | copy-start | bytes 3145732 | tf_op jit(solution)/shard_map/while/body/eval_jaxpr/cond
  500.0 9.2 %copy-start.4 = (bf16[1024,512]{0,1:T(8,128)(2,1)S(1)}, bf16[1024,512]{0,1:T(8,128)(2,1)}, u32[]{:S(2)}) copy-start(bf16[1024,512]{0,1:T(8,128)(2,1)} %copy-done.3) | copy-start | bytes 3145732 | tf_op jit(solution)/shard_map/while/body/eval_jaxpr/cond
  531.2 6.0 %copy-start.6 = (f32[4096]{0:T(1024)S(1)}, f32[4096]{0:T(1024)}, u32[]{:S(2)}) copy-start(f32[4096]{0:T(1024)} %param.25) | copy-start | bytes 49156
  531.2 7.9 %copy-start.1 = (bf16[768,384]{1,0:T(8,128)(2,1)S(1)}, bf16[768,384]{1,0:T(8,128)(2,1)}, u32[]{:S(2)}) copy-start(bf16[768,384]{1,0:T(8,128)(2,1)} %param.22) | copy-start | bytes 1769476
  (4 other events, 3.9 us)
Sparse Core Ops, SparseCore 0:
  14.1 18.8 all-gather.3
  34.5 19.9 all-gather.7
  56.6 147.6 all-gather.5
